TPU v7x, 32 devices: a whole 2x2x4 slice. The times are simulated.
32 devices in a mesh: grp: 2 (over x), sp: 4 (over z), tp: 4 (over y, core).
Axes of the slice: x: 2, y: 2, z: 4, core: 2. Of those that a mesh axis runs over, the one named last changes fastest.
Arguments:
- tokens: bfloat16 [4, 1024, 2048], P('grp', 'sp'), parts along dimension 0, may hold values from -6 to 6
- decoded_input: bfloat16 [4, 2048], P('grp'), parts along dimension 0, may hold values from -6 to 6
- query_weight: bfloat16 [2048, 4096], P(None, 'tp'), may hold values from -0.125 to 0.125
- key_weight: bfloat16 [2048, 4096], P(None, 'tp'), may hold values from -0.125 to 0.125
- value_weight: bfloat16 [2048, 4096], P(None, 'tp'), may hold values from -0.125 to 0.125
- gate_weight: bfloat16 [2048, 2, 32], replicated, may hold values from -0.125 to 0.125
- head_decay_rate: float32 [32], P('tp'), may hold values from 9.765625e-05 to 0.08, as said below
- extra_log_decay: float32 [4, 32, 1024], P('grp', 'tp', 'sp'), parts along dimension 0, may hold values from -2.8 to 0, as said below
- read_norm_gain: float32 [128], replicated, may hold values from 0.1 to 1.9
Outputs:
- cache: bfloat16 [4, 32, 128, 128], P('grp', 'tp', 'sp'), parts along dimension 0
- read: bfloat16 [4, 4096], P('grp', 'tp'), parts along dimension 0
There are 2 independent parts, one for each index of `grp`. A program takes and returns all parts, laid end to end along the dimension named above; an argument that names none is the same for every part. Nothing has to cross between parts.
Inputs may be any that keep to these rules, and one draw needn't show every extreme that they name: `head_decay_rate`: positive. `extra_log_decay`: zero at all but a few positions.
All inputs are finite; a program needn't handle non-finite values.
Results may differ from a plain program's by a relative error of at most 0.002.
Values sent between devices are 32-bit elements; how exact they have to be, the bound alone decides.
A program may use at most 64 MiB of HBM per device.

v0:
```python
import jax
import jax.numpy as jnp
from jax import lax
from jax.sharding import PartitionSpec as P

BLOCK = 64


epsilon = 1e-06
write_offset = 5.0
highest = lax.Precision.HIGHEST


def prefix(shard, axis, combine, identity):
    size, mine = (lax.axis_size(axis), lax.axis_index(axis))
    everything = lax.all_gather(shard, axis)
    start = jnp.broadcast_to(jnp.asarray(identity, shard.dtype), shard.shape)

    def lap(k, before):
        at = size - 1 - k
        reached = at > mine
        new = combine(before, everything[at])
        return jnp.where(reached, new, before)

    return lax.fori_loop(0, size, lap, start)


def unit_rows(vectors):
    return vectors * lax.rsqrt(jnp.sum(vectors * vectors, axis=-1, keepdims=True) + epsilon)


def project(flat, key_weight, value_weight, gate_cols, head_decay_rate, head_total, head_dim):
    keys = jax.nn.silu(jnp.dot(flat, key_weight, preferred_element_type=jnp.float32))
    keys = unit_rows(keys.reshape(flat.shape[0], head_total, head_dim))
    values = jax.nn.silu(jnp.dot(flat, value_weight, preferred_element_type=jnp.float32))
    values = values.reshape(flat.shape[0], head_total, head_dim)
    gates = jnp.dot(flat, gate_cols, preferred_element_type=jnp.float32)
    beta = jax.nn.sigmoid(gates[:, :head_total] - write_offset)
    decay_factor = -head_decay_rate * jax.nn.softplus(gates[:, head_total:])
    return (keys, values, beta, decay_factor)


def block_parts(keys, values, beta, decay_factor):
    size = keys.shape[-2]
    head_dim = values.shape[-1]
    running = jnp.cumsum(decay_factor, axis=-1)
    index = jnp.arange(size)
    strict = index[:, None] > index[None, :]
    spread = running[..., :, None] - running[..., None, :]
    below = jnp.where(strict, jnp.exp(jnp.where(strict, spread, 0.0)), 0.0)
    inner = jnp.einsum("...id,...jd->...ij", keys, keys, precision=highest)
    lower = jnp.eye(size, dtype=jnp.float32) + beta[..., :, None] * inner * below
    right = jnp.concatenate(
        [values * beta[..., None], keys * (beta * jnp.exp(running))[..., None]], axis=-1
    )
    solved = jax.scipy.linalg.solve_triangular(lower, right, lower=True, unit_diagonal=True)
    total = jnp.exp(running[..., -1])
    carried = keys * jnp.exp(running[..., -1:] - running)[..., None]
    return (solved[..., :head_dim], solved[..., head_dim:], total, carried)


def product(left, right):
    return jnp.einsum("shij,shjk->shik", left, right, precision=highest)


def finish(
    state_rows,
    key_rows,
    key_read,
    query_read,
    query,
    new_key,
    new_value,
    new_beta,
    keep,
    read_norm_gain,
):
    intersection = jnp.sum(query * new_key, axis=-1)
    cache = (
        keep[..., None, None] * state_rows
        - (keep * new_beta)[..., None, None] * key_rows[..., :, None] * key_read[..., None, :]
        + new_beta[..., None, None] * key_rows[..., :, None] * new_value[..., None, :]
    )
    mixed = (
        keep[..., None] * query_read
        - (keep * new_beta * intersection)[..., None] * key_read
        + (new_beta * intersection)[..., None] * new_value
    )
    normed = (
        mixed
        * lax.rsqrt(jnp.mean(mixed * mixed, axis=-1, keepdims=True) + epsilon)
        * read_norm_gain
    )
    sequence_total = normed.shape[0]
    return (cache.astype(jnp.bfloat16), normed.reshape(sequence_total, -1).astype(jnp.bfloat16))


def per_device(
    tokens,
    decoded_input,
    query_weight,
    key_weight,
    value_weight,
    gate_weight,
    head_decay_rate,
    extra_log_decay,
    read_norm_gain,
):
    sequence_total, batch_rows, width = tokens.shape
    local_heads = head_decay_rate.shape[0]
    head_dim = key_weight.shape[1] // local_heads
    first_head = lax.axis_index("tp") * local_heads
    gate_cols = lax.dynamic_slice_in_dim(gate_weight, first_head, local_heads, 2).reshape(
        width, 2 * local_heads
    )
    flat = tokens.reshape(sequence_total * batch_rows, width)
    keys, values, beta, decay_factor = project(
        flat, key_weight, value_weight, gate_cols, head_decay_rate, local_heads, head_dim
    )
    count = batch_rows // BLOCK
    keys_b = keys.reshape(sequence_total, count, BLOCK, local_heads, head_dim).transpose(
        0, 3, 1, 2, 4
    )
    values_b = values.reshape(sequence_total, count, BLOCK, local_heads, head_dim).transpose(
        0, 3, 1, 2, 4
    )
    beta_b = beta.reshape(sequence_total, count, BLOCK, local_heads).transpose(0, 3, 1, 2)
    decay_every_token = (
        decay_factor.reshape(sequence_total, batch_rows, local_heads).transpose(0, 2, 1)
        + extra_log_decay
    )
    decay_b = decay_every_token.reshape(sequence_total, local_heads, count, BLOCK)
    solved_u, solved_w, total, carried = block_parts(keys_b, values_b, beta_b, decay_b)
    square = jnp.eye(head_dim, dtype=jnp.float32)
    change = total[..., None, None] * square - jnp.einsum(
        "shncd,shnce->shnde", carried, solved_w, precision=highest
    )
    push = jnp.einsum("shncd,shncv->shndv", carried, solved_u, precision=highest)

    def compose(carry, block):
        return ((product(block[0], carry[0]), product(block[0], carry[1]) + block[1]), None)

    identity = jnp.broadcast_to(square, (sequence_total, local_heads, head_dim, head_dim))
    empty = jnp.zeros((sequence_total, local_heads, head_dim, head_dim), jnp.float32)
    (trans_a, trans_b), _ = lax.scan(
        compose, (identity, empty), (jnp.moveaxis(change, 2, 0), jnp.moveaxis(push, 2, 0))
    )
    query = jax.nn.silu(
        jnp.dot(decoded_input, query_weight, preferred_element_type=jnp.float32)
    ).reshape(sequence_total, local_heads, head_dim)
    new_key, new_value, new_beta, new_decay = project(
        decoded_input, key_weight, value_weight, gate_cols, head_decay_rate, local_heads, head_dim
    )
    keep = jnp.exp(new_decay)
    row_count = head_dim // lax.axis_size("sp")
    row_start = lax.axis_index("sp") * row_count
    key_rows = lax.dynamic_slice_in_dim(new_key, row_start, row_count, 2)

    def multiply(earlier, later):
        return product(earlier, later)

    after = prefix(trans_a, "sp", multiply, identity)
    shares = product(after, trans_b)
    state_rows = lax.psum_scatter(shares, "sp", scatter_dimension=2, tiled=True)
    query_rows = lax.dynamic_slice_in_dim(query, row_start, row_count, 2)
    partial_key = jnp.einsum("shd,shdv->shv", key_rows, state_rows, precision=highest)
    partial_query = jnp.einsum("shd,shdv->shv", query_rows, state_rows, precision=highest)
    key_read, query_read = lax.psum((partial_key, partial_query), "sp")
    return finish(
        state_rows,
        key_rows,
        key_read,
        query_read,
        query,
        new_key,
        new_value,
        new_beta,
        keep,
        read_norm_gain,
    )


def solution(mesh):
    in_specs = (
        P("grp", "sp", None),
        P("grp", None),
        P(None, "tp"),
        P(None, "tp"),
        P(None, "tp"),
        P(),
        P("tp"),
        P("grp", "tp", "sp"),
        P(),
    )
    out_specs = (P("grp", "tp", "sp", None), P("grp", "tp"))
    return jax.shard_map(
        per_device, mesh=mesh, in_specs=in_specs, out_specs=out_specs, check_vma=False
    )
```

profile of v0, /device:TPU:0, one launch (start us, length us, event | category | flops | bytes accessed | tf_op | source)
XLA Modules:
  0.0 565.8 jit_solution(6733317323683828225)
XLA Ops:
  12.7 6.1 %multiply_bitcast_fusion.1 = (f32[64,8,8,128]{3,1,2,0:T(8,128)S(1)}, f32[64,8,8,128]{3,1,2,0:T(8,128)}) fusion(bf16[512,2048]{1,0:T(8,128)(2,1)S(1)} %bitcast.148, bf16[2048,1024]{1,0:T(8,128)(2,1)} %param.16), kind=kOutput, calls=%fused_computation.34 | convolution fusion | flops 2150105088 | bytes 10485760 | tf_op jit(solution)/shard_map/dot_general | solution.py:33
  25.9 2.6 multiply_bitcast_fusion
  30.3 5.7 %add_bitcast_fusion = f32[2,8,4,1,64,64]{5,4,3,2,1,0:T(8,128)} fusion(f32[2,4,64,8,128]{4,3,2,1,0:T(8,128)S(1)} %bitcast.150, f32[64,64]{1,0:T(8,128)S(1)} %get-tuple-element.236, f32[2,8,4,64]{3,2,1,0:T(4,128)S(1)} %copy.77, f32[2,8,4,64]{3,2,1,0:T(4,128)S(1)} %copy.76, f32[64,64]{1,0:T(8,128)S(1)} %get-tuple-element.235, ...), kind=kOutput, calls=%fused_computation.33 | convolution fusion | flops 405274624 | bytes 3235840 | tf_op jit(solution)/shard_map/...id,...jd->...ij/dot_general | solution.py:51
  36.1 316.0 %custom-call.4 = f32[2,8,4,1,64,64]{4,5,3,2,1,0:T(8,128)} custom-call(f32[2,8,4,1,64,64]{5,4,3,2,1,0:T(8,128)} %add_bitcast_fusion), custom_call_target="InvertDiagBlocksLowerTriangular" | custom-call | tf_op jit(solution)/shard_map/jit(_solve_triangular)/vmap(vmap(vmap()))/triangular_solve | solution.py:56
  352.1 3.7 bitcast_multiply_fusion
  355.8 4.3 fusion.15
  360.2 9.5 %convolution_bitcast_fusion.1 = f32[4,2,8,128,128]{4,3,0,2,1:T(8,128)} fusion(f32[2,8,4,64,256]{4,3,2,1,0:T(8,128)S(1)} %fusion.15, f32[2,4,64,8,128]{4,3,2,1,0:T(8,128)S(1)} %bitcast.152, f32[2,8,4,64]{3,2,1,0:T(4,128)S(1)} %copy.74, f32[2,4,64,8]{2,1,0,3:T(4,128)S(1)} %rsqrt.28), kind=kOutput, calls=%fused_computation.22 | convolution fusion | flops 806354944 | bytes 8454144 | tf_op jit(solution)/shard_map/shncd,shncv->shndv/dot_general | solution.py:138
  369.7 9.8 %bitcast_subtract_fusion = f32[4,2,8,128,128]{4,3,0,2,1:T(8,128)} fusion(f32[2,8,4,64,256]{4,3,2,1,0:T(8,128)S(1)} %fusion.15, f32[128,128]{1,0:T(8,128)S(1)} %fusion.34, f32[4,2,8]{0,2,1:T(8,128)S(1)} %copy.70, f32[2,4,64,8,128]{4,3,2,1,0:T(8,128)S(1)} %bitcast.153, f32[2,8,4,64]{3,2,1,0:T(4,128)S(1)} %copy.74, f32[2,4,64,8]{2,1,0,3:T(4,128)S(1)} %rsqrt.28), kind=kOutput, calls=%fused_computation.21 | convolution fusion | flops 808452096 | bytes 8527872 | tf_op jit(solution)/shard_map/shncd,shnce->shnde/dot_general | solution.py:135
  379.5 29.9 %while.29 = (s32[]{:T(128)}, f32[2,8,128,128]{3,2,1,0:T(8,128)S(1)}, f32[2,8,128,128]{3,2,1,0:T(8,128)}, f32[4,2,8,128,128]{4,3,0,2,1:T(8,128)}, f32[4,2,8,128,128]{4,3,0,2,1:T(8,128)}, /*index=5*/s32[]{:T(128)}, s32[]{:T(128)}) while((s32[]{:T(128)}, f32[2,8,128,128]{3,2,1,0:T(8,128)S(1)}, f32[2,8,128,128]{3,2,1,0:T(8,128)}, ...), condition=%wide.region_3.4_spmd.clone, body=%wide.region_2.3_spmd.clone.sunk | while | flops 805830656 | bytes 11535959 | solution.py:145
  380.8 3.7 convolution_add_fusion.2
  388.3 3.7 convolution_add_fusion.2
  395.7 3.7 convolution_add_fusion.2
  403.2 3.7 convolution_add_fusion.2
  410.6 2.8 fusion.57
  413.5 80.6 %all-gather.3.cloned.1.call-done = f32[8,8,128,128]{3,2,1,0:T(8,128)} async-done(((f32[2,8,128,128]{3,2,1,0:T(8,128)}), f32[8,8,128,128]{3,2,1,0:T(8,128)}) %all-gather.3.cloned.1.call-update) | async-done | bytes 4194320 | tf_op jit(solution)/shard_map/all_gather | solution.py:16
  494.2 13.2 %while.28 = (s32[]{:T(128)}, f32[2,8,128,128]{2,3,1,0:T(8,128)S(1)}, s32[]{:T(128)}, f32[4,2,8,128,128]{4,3,2,1,0:T(8,128)}, s32[]{:T(128)}, /*index=5*/s32[]{:T(128)}, s32[]{:T(128)}, s32[]{:T(128)}) while((s32[]{:T(128)}, f32[2,8,128,128]{2,3,1,0:T(8,128)S(1)}, s32[]{:T(128)}, f32[4,2,8,128,128]{4,3,2,1,0:T(8,128)}, s32[]{:T(128)}, ...), condition=%wide.region_5.6_spmd, body=%wide.region_4.5_spmd.sunk | while | flops 402915328 | bytes 6291601 | solution.py:25
  494.5 3.1 fusion.94
  497.8 3.1 fusion.94
  501.0 3.1 fusion.94
  504.3 3.1 fusion.94
  507.4 4.0 fusion.56
  511.5 3.0 fusion.45
  516.8 20.6 %reduce-scatter.2.cloned.1.call-done = f32[2,8,32,128]{3,2,1,0:T(8,128)} async-done(((f32[2,8,128,128]{3,2,1,0:T(8,128)}), f32[2,8,32,128]{3,2,1,0:T(8,128)}) %reduce-scatter.2.cloned.1.call-update) | async-done | bytes 262160 | tf_op jit(solution)/shard_map/reduce_scatter | solution.py:164
  540.0 16.3 %all-reduce = (f32[2,8,128]{2,1,0:T(8,128)S(1)}, f32[2,8,128]{2,1,0:T(8,128)S(1)}) all-reduce(f32[2,8,128]{2,1,0:T(8,128)S(1)} %bitcast.161, f32[2,8,128]{2,1,0:T(8,128)S(1)} %bitcast.162), channel_id=1, replica_groups=mesh['grp'=2,'sp'=4,'tp'=4] {'sp'}, use_global_device_ids=true, to_apply=%region_8.9 | all-reduce | flops 4096 | bytes 32768 | tf_op jit(solution)/shard_map/psum | solution.py:168
  (91 shorter events, 38.2 us)
Async XLA Ops:
  7.2 1.6 copy-start
  7.2 3.2 copy-start.8
  7.2 486.9 %all-gather.3.cloned.1.call-start = ((), (), s32[]{:S(2)}) async-start(), calls=%async_computation.2 | async-start | bytes 5242880 | tf_op jit(solution)/shard_map/all_gather | solution.py:16
  23.0 2.8 copy-start.4
  25.9 4.5 copy-start.2
  352.1 3.7 copy-start.6
  355.8 4.3 copy-start.3
  379.5 31.1 %copy-start.7 = (bf16[2,2048]{1,0:T(2,128)(2,1)S(1)}, bf16[2,2048]{1,0:T(2,128)(2,1)}, u32[]{:S(2)}) copy-start(bf16[2,2048]{1,0:T(2,128)(2,1)} %param.14) | copy-start | bytes 24580
  409.5 1.0 copy-start.1
  410.5 127.0 %reduce-scatter.2.cloned.1.call-start = ((), (), s32[]{:S(2)}) async-start(), calls=%async_computation.1 | async-start | bytes 1310720 | tf_op jit(solution)/shard_map/reduce_scatter | solution.py:164
  511.5 4.4 copy-start.5
  515.9 40.6 %copy-start.9 = (f32[128]{0:T(128)S(1)}, f32[128]{0:T(128)}, u32[]{:S(2)}) copy-start(f32[128]{0:T(128)} %param.21) | copy-start | bytes 1540
Sparse Core Ops, SparseCore 0:
  410.6 83.4 all-gather.2
  511.6 25.7 reduce-scatter.1
where the time goes:
time: 567 us; the launch traced here: 566 us
  other arithmetic  327 us (58%)
  waiting for transfers between devices  101 us (18%)
  matrix products  90.6 us (16%)
  blocking collectives  16.3 us (3%)
  local copies, waits for them, and re-layouts  15.3 us (3%)
  between operations  14.4 us (3%)
    another operation x2, other arithmetic, block_parts(): jax.scipy.linalg.solve_triangular(lower, right, lower=True, unit_diagonal...  316 us
    all_gather x1, waiting for transfers between devices, prefix(): everything = lax.all_gather(shard, axis)  80.6 us
    dot_general x13, matrix products, product(): return jnp.einsum('shij,shjk->shik', left, right, precision=highest)  41.1 us
    reduce_scatter x1, waiting for transfers between devices, per_device(): state_rows = lax.psum_scatter(shares, 'sp', scatter_dimension=2, tiled=True)  20.6 us
    psum x1, blocking collectives, per_device(): key_read, query_read = lax.psum((partial_key, partial_query), 'sp')  16.3 us
  transfers between devices with their start and end apart: 2, of which 2 were waited for; matrix products, arithmetic and copies ran while one was open for 1% of the time, Pallas kernels for 0%

commit v1 on v0

v1 whole, which is shorter than its diff:
```python
import functools

import jax
import jax.numpy as jnp
from jax import lax
from jax.experimental import pallas as pl
from jax.experimental.pallas import tpu as pltpu
from jax.sharding import PartitionSpec as P

epsilon = 1e-06
write_offset = 5.0
f32 = jnp.float32
bf16 = jnp.bfloat16
MESH = pl.DeviceIdType.MESH
ROWS = (((1,), (0,)), ((), ()))
SAME = (((1,), (1,)), ((), ()))
OUTER = (((0,), (0,)), ((), ()))


def dot(a, b, dims=ROWS):
    return lax.dot_general(a, b, dims, preferred_element_type=f32)


def split(x):
    high = x.astype(bf16)
    return high, (x - high.astype(f32)).astype(bf16)


def dot3(a, b, dims=ROWS):
    ah, al = a
    bh, bl = b
    return dot(ah, bh, dims) + (dot(ah, bl, dims) + dot(al, bh, dims))


def silu(x):
    return x * jax.nn.sigmoid(x)


def unit_rows(x):
    return x * lax.rsqrt(jnp.sum(x * x, axis=-1, keepdims=True) + epsilon)


def span_solve(lower, right):
    size = lower.shape[0]
    row = lax.broadcasted_iota(jnp.int32, (size, size), 0)
    col = lax.broadcasted_iota(jnp.int32, (size, size), 1)
    eye = jnp.where(row == col, 1.0, 0.0)
    inverse = eye - jnp.where((row % 2 == 1) & (col == row - 1), lower, 0.0)
    width = 2
    while width < size:
        pick = (row // width % 2 == 1) & (col // width == row // width - 1)
        part = jnp.where(pick, lower, 0.0).astype(bf16)
        coarse = inverse.astype(bf16)
        inverse = inverse - dot(coarse, dot(part, coarse).astype(bf16))
        width *= 2
    coarse = inverse.astype(bf16)
    first = dot(coarse, right.astype(bf16))
    residual = (right - first) - dot3(split(lower), split(first))
    return first + dot(coarse, residual.astype(bf16))


def kernel(
    parts,
    tok,
    dec,
    kw,
    vw,
    qw,
    gates_t,
    rate,
    extra,
    gain,
    cache_o,
    read_o,
    x,
    rows_s,
    cols_s,
    decg,
    a_buf,
    b_buf,
    d_buf,
    s_recv,
    s_send,
    fin,
    rfin,
    tok_sem,
    s_send_sem,
    s_recv_sem,
    f_send_sem,
    f_recv_sem,
):
    groups = a_buf.shape[0]
    seqs, span, width = tok.shape
    total_rows = seqs * span
    head_dim = kw.shape[1]
    padded = rate.shape[0]
    share = head_dim // parts
    step = pl.program_id(0)
    me = lax.axis_index("sp")
    last = parts - 1
    barrier = pltpu.get_barrier_semaphore()

    @pl.when(step == 0)
    def _():
        for other in range(parts):

            @pl.when(me != other)
            def _():
                pl.semaphore_signal(
                    barrier, inc=1, device_id={"sp": other}, device_id_type=MESH
                )

        loads = [
            pltpu.make_async_copy(tok.at[s], x.at[pl.ds(s * span, span)], tok_sem.at[s])
            for s in range(seqs)
        ]
        for load in loads:
            load.start()
        x[total_rows:, :] = jnp.zeros((x.shape[0] - total_rows, width), bf16)
        x[total_rows : total_rows + seqs, :] = dec[...]
        for load in loads:
            load.wait()
        gates = dot(gates_t[...], x[...], SAME)
        beta = jax.nn.sigmoid(gates[:padded] - write_offset)
        raw = gates[padded:]
        soft = jnp.maximum(raw, 0.0) + jnp.log1p(jnp.exp(-jnp.abs(raw)))
        decay = -rate[...] * soft
        decg[:padded, :] = beta[:, total_rows:]
        decg[padded:, :] = jnp.exp(decay[:, total_rows:])
        row = lax.broadcasted_iota(jnp.int32, (span, span), 0)
        col = lax.broadcasted_iota(jnp.int32, (span, span), 1)
        upto = jnp.where(row <= col, 1.0, 0.0).astype(bf16)
        for s in range(seqs):
            mine = decay[:, s * span : (s + 1) * span] + extra[s]
            high, rest = split(mine)
            rest_f = mine - high.astype(f32)
            low = (rest_f - rest.astype(f32)).astype(bf16)
            running = dot(high, upto) + (dot(rest, upto) + dot(low, upto))
            rows_s[:padded, s * span : (s + 1) * span] = beta[:, s * span : (s + 1) * span]
            rows_s[padded : 2 * padded, s * span : (s + 1) * span] = running
        rows_s[2 * padded :, :] = jnp.zeros((rows_s.shape[0] - 2 * padded, total_rows), f32)
        cols_s[...] = rows_s[...].T
        pl.semaphore_wait(barrier, parts - 1)

    @pl.when(step < groups)
    def _():
        weights = jnp.concatenate([kw[...], vw[...]], axis=1)
        used = total_rows + 16
        both = silu(dot(x[:used, :], weights))
        keys = unit_rows(both[:, :head_dim])
        values = both[:, head_dim:]
        query = silu(dot(x[total_rows:used, :], qw[...]))
        lane = lax.broadcasted_iota(jnp.int32, (span, cols_s.shape[1]), 1)
        row = lax.broadcasted_iota(jnp.int32, (span, span), 0)
        col = lax.broadcasted_iota(jnp.int32, (span, span), 1)
        strict = row > col
        hrow = lax.broadcasted_iota(jnp.int32, (head_dim, head_dim), 0)
        hcol = lax.broadcasted_iota(jnp.int32, (head_dim, head_dim), 1)
        for s in range(seqs):
            at = total_rows + s
            d_buf[step, s, 0:1, :] = keys[at : at + 1]
            d_buf[step, s, 1:2, :] = query[s : s + 1]
            d_buf[step, s, 2:3, :] = values[at : at + 1]
            k = keys[s * span : (s + 1) * span]
            v = values[s * span : (s + 1) * span]
            table = cols_s[s * span : (s + 1) * span, :]
            beta = jnp.sum(jnp.where(lane == step, table, 0.0), axis=1, keepdims=True)
            run = jnp.sum(
                jnp.where(lane == padded + step, table, 0.0), axis=1, keepdims=True
            )
            run_row = rows_s[pl.ds(padded + step, 1), s * span : (s + 1) * span]
            end = run[span - 1 :, :]
            spread = jnp.where(strict, run - run_row, 0.0)
            below = jnp.where(strict, jnp.exp(spread), 0.0)
            kk = split(k)
            lower = beta * dot3(kk, kk, SAME) * below
            right = jnp.concatenate([v * beta, k * (beta * jnp.exp(run))], axis=1)
            solved = span_solve(lower, right)
            carried = (k * jnp.exp(end - run)).T
            moved = dot3(split(carried), split(solved))
            b_buf[step, s] = moved[:, :head_dim]
            a_buf[step, s] = (
                jnp.where(hrow == hcol, jnp.exp(end), 0.0) - moved[:, head_dim:]
            )

    def state_copy(c, right):
        return pltpu.make_async_remote_copy(
            src_ref=s_send.at[c],
            dst_ref=s_recv.at[c],
            send_sem=s_send_sem.at[c],
            recv_sem=s_recv_sem.at[c],
            device_id={"sp": right},
            device_id_type=MESH,
        )

    def share_copy(c, to):
        return pltpu.make_async_remote_copy(
            src_ref=fin.at[c, to],
            dst_ref=rfin.at[c],
            send_sem=f_send_sem.at[c, to],
            recv_sem=f_recv_sem.at[c],
            device_id={"sp": to},
            device_id_type=MESH,
        )

    group = step - me
    busy = (group >= 0) & (group < groups)
    right_of = jnp.minimum(me + 1, last)

    @pl.when(busy & (me == 0))
    def _():
        s_send[group] = b_buf[group]
        state_copy(group, right_of).start()

    def advance(s):
        return dot3(split(a_buf[group, s]), split(s_recv[group, s])) + b_buf[group, s]

    @pl.when(busy & (me > 0) & (me < last))
    def _():
        state_copy(group, right_of).wait_recv()
        for s in range(seqs):
            s_send[group, s] = advance(s)
        state_copy(group, right_of).start()

    @pl.when(busy & (me == last))
    def _():
        state_copy(group, 0).wait_recv()
        eight = lax.broadcasted_iota(jnp.int32, (8, head_dim), 0)
        for s in range(seqs):
            final = advance(s)
            rows = d_buf[group, s]
            new_key, query, new_value = rows[0:1], rows[1:2], rows[2:3]
            reads = dot3(split(rows), split(final))
            key_read, query_read = reads[0:1], reads[1:2]
            beta = decg[pl.ds(group, 1), s : s + 1]
            keep = decg[pl.ds(padded + group, 1), s : s + 1]
            meet = jnp.sum(query * new_key, axis=-1, keepdims=True)
            delta = beta * new_value - (keep * beta) * key_read
            key_pad = jnp.where(eight == 0, new_key, 0.0)
            delta_pad = jnp.where(eight == 0, delta, 0.0)
            outer = dot3(split(key_pad), split(delta_pad), OUTER)
            state = keep * final + outer
            mixed = (
                keep * query_read
                - (keep * beta * meet) * key_read
                + (beta * meet) * new_value
            )
            normed = (
                mixed
                * lax.rsqrt(jnp.mean(mixed * mixed, axis=-1, keepdims=True) + epsilon)
                * gain[...]
            )
            normed = jnp.broadcast_to(normed, (8, head_dim))
            for to in range(last):
                fin[group, to, s, :share] = state[to * share : (to + 1) * share]
                fin[group, to, s, share:] = normed
            rfin[group, s, :share] = state[last * share :]
            rfin[group, s, share:] = normed
        for to in range(last):
            share_copy(group, to).start()

    @pl.when(step == groups - 1 + last)
    def _():
        @pl.when(me < last)
        def _():
            for c in range(groups):
                state_copy(c, right_of).wait_send()
                share_copy(c, 0).wait_recv()

        @pl.when(me == last)
        def _():
            for c in range(groups):
                for to in range(last):
                    share_copy(c, to).wait_send()

        for c in range(groups):
            for s in range(seqs):
                cache_o[s, c] = rfin[c, s, :share].astype(bf16)
                read_o[s : s + 1, c * head_dim : (c + 1) * head_dim] = rfin[
                    c, s, share : share + 1
                ].astype(bf16)


def per_device(
    parts,
    tokens,
    decoded_input,
    query_weight,
    key_weight,
    value_weight,
    gate_weight,
    head_decay_rate,
    extra_log_decay,
    read_norm_gain,
):
    seqs, span, width = tokens.shape
    heads = head_decay_rate.shape[0]
    head_dim = key_weight.shape[1] // heads
    share = head_dim // parts
    padded = -(-heads // 8) * 8
    first = lax.axis_index("tp") * heads
    gates = lax.dynamic_slice_in_dim(gate_weight, first, heads, 2)
    gates = gates.transpose(1, 2, 0)
    more = padded - heads
    if more:
        gates = jnp.pad(gates, ((0, 0), (0, more), (0, 0)))
        extra_log_decay = jnp.pad(extra_log_decay, ((0, 0), (0, more), (0, 0)))
        head_decay_rate = jnp.pad(head_decay_rate, (0, more))
    gates = gates.reshape(2 * padded, width)
    table = max(128, 2 * padded)
    whole = pl.BlockSpec(memory_space=pltpu.VMEM)
    cut = pl.BlockSpec((width, head_dim), lambda t: (0, jnp.minimum(t, heads - 1)))
    block = (heads, seqs, head_dim, head_dim)
    return pl.pallas_call(
        functools.partial(kernel, parts),
        grid=(heads + parts - 1,),
        out_shape=(
            jax.ShapeDtypeStruct((seqs, heads, share, head_dim), bf16),
            jax.ShapeDtypeStruct((seqs, heads * head_dim), bf16),
        ),
        in_specs=[pl.BlockSpec(memory_space=pl.ANY), whole, cut, cut, cut]
        + [whole] * 4,
        out_specs=(whole, whole),
        scratch_shapes=[
            pltpu.VMEM((seqs * span + 128, width), bf16),
            pltpu.VMEM((table, seqs * span), f32),
            pltpu.VMEM((seqs * span, table), f32),
            pltpu.VMEM((2 * padded, 128), f32),
            pltpu.VMEM(block, f32),
            pltpu.VMEM(block, f32),
            pltpu.VMEM((heads, seqs, 8, head_dim), f32),
            pltpu.VMEM(block, f32),
            pltpu.VMEM(block, f32),
            pltpu.VMEM((heads, parts, seqs, share + 8, head_dim), f32),
            pltpu.VMEM((heads, seqs, share + 8, head_dim), f32),
            pltpu.SemaphoreType.DMA((seqs,)),
            pltpu.SemaphoreType.DMA((heads,)),
            pltpu.SemaphoreType.DMA((heads,)),
            pltpu.SemaphoreType.DMA((heads, parts)),
            pltpu.SemaphoreType.DMA((heads,)),
        ],
        compiler_params=pltpu.CompilerParams(
            collective_id=0,
            has_side_effects=True,
            dimension_semantics=("arbitrary",),
            vmem_limit_bytes=48 * 1024 * 1024,
        ),
    )(
        tokens,
        decoded_input,
        key_weight,
        value_weight,
        query_weight,
        gates,
        head_decay_rate.reshape(padded, 1),
        extra_log_decay,
        read_norm_gain.reshape(1, head_dim),
    )


def solution(mesh):
    in_specs = (
        P("grp", "sp", None),
        P("grp", None),
        P(None, "tp"),
        P(None, "tp"),
        P(None, "tp"),
        P(),
        P("tp"),
        P("grp", "tp", "sp"),
        P(),
    )
    out_specs = (P("grp", "tp", "sp", None), P("grp", "tp"))
    return jax.shard_map(
        functools.partial(per_device, mesh.shape["sp"]),
        mesh=mesh,
        in_specs=in_specs,
        out_specs=out_specs,
        check_vma=False,
    )
```

time: 567 us -> 101 us (0.18)
  other arithmetic: 327 us -> 0 us
  waiting for transfers between devices: 101 us -> 0 us
  Pallas kernels: 0 us -> 94.6 us
  matrix products: 90.6 us -> 0 us
  blocking collectives: 16.3 us -> 0 us
  between operations: 14.4 us -> 0.66 us
  local copies, waits for them, and re-layouts: 15.3 us -> 5.87 us
    another operation x3 -> x0, other arithmetic: 318 us -> none  [the longest x2 316 us: block_parts(): jax.scipy.linalg.solve_triangular(lower, right, lower=True, unit_diagonal...]
    pallas_call x0 -> x1, Pallas kernels: none -> 94.6 us  [per_device(): pl.pallas_call(functools.partial(kernel, parts), grid=(heads + parts - 1,...]
    dot_general x25 -> x0, matrix products: 86.3 us -> none  [the longest x13 41.1 us: product(): return jnp.einsum('shij,shjk->shik', left, right, precision=highest)]
    all_gather x1 -> x0, waiting for transfers between devices: 80.6 us -> none  [prefix(): everything = lax.all_gather(shard, axis)]
    reduce_scatter x1 -> x0, waiting for transfers between devices: 20.6 us -> none  [per_device(): state_rows = lax.psum_scatter(shares, 'sp', scatter_dimension=2, tiled=True)]
    psum x1 -> x0, blocking collectives: 16.3 us -> none  [per_device(): key_read, query_read = lax.psum((partial_key, partial_query), 'sp')]
  transfers between devices with their start and end apart: 2 -> 0, of which waited for: 2 -> 0; matrix products, arithmetic and copies ran while one was open for 1% -> 0% of each run, Pallas kernels for 0% -> 0%
where the time goes in v1:
time: 101 us
  Pallas kernels  94.6 us (94%)
  local copies, waits for them, and re-layouts  5.87 us (6%)
    pallas_call x1, Pallas kernels, per_device(): pl.pallas_call(functools.partial(kernel, parts), grid=(heads + parts - 1,...  94.6 us
    unnamed x12, local copies, waits for them, and re-layouts  5.1 us

profile of v1, /device:TPU:0, one launch (start us, length us, event | category | flops | bytes accessed | tf_op | source)
XLA Modules:
  0.0 101.1 jit_solution(1645381740333243568)
XLA Ops:
  0.6 0.0 copy-start
  0.6 0.8 copy.11.rate
  1.4 0.2 copy-done
  1.6 0.0 copy-start.1
  1.6 1.6 %copy-done.1 = bf16[2,256,2048]{2,1,0:T(8,128)(2,1)S(1)} copy-done((bf16[2,256,2048]{2,1,0:T(8,128)(2,1)S(1)}, bf16[2,256,2048]{2,1,0:T(8,128)(2,1)}, u32[]{:S(2)}) %copy-start.1) | copy-done | bytes 2097176
  3.2 0.0 copy-start.2
  3.2 0.7 copy-done.2
  3.9 0.0 copy-start.3
  3.9 0.7 copy-done.3
  4.6 0.0 copy-start.4
  4.6 0.7 copy-done.4
  5.3 94.6 %shard_map.104 = (bf16[2,8,32,128]{3,2,1,0:T(8,128)(2,1)S(1)}, bf16[2,1024]{1,0:T(2,128)(2,1)S(1)}) custom-call(bf16[2,256,2048]{2,1,0:T(8,128)(2,1)S(1)} %copy-done.1, bf16[2,2048]{1,0:T(2,128)(2,1)S(1)} %copy-done.3, bf16[2048,1024]{1,0:T(8,128)(2,1)} %kw.1, bf16[2048,1024]{1,0:T(8,128)(2,1)} %vw.1, bf16[2048,1024]{1,0:T(8,128)(2,1)} %qw.1, ...), custom_call_target="tpu_custom_call" | custom-call | tf_op jit(solution)/shard_map/pallas_call | solution.py:314
  99.9 0.7 copy.14
  100.6 0.6 copy.15
  (1 shorter events, 0.0 us)
Async XLA Ops:
  0.6 1.0 copy-start
  1.6 1.6 %copy-start.1 = (bf16[2,256,2048]{2,1,0:T(8,128)(2,1)S(1)}, bf16[2,256,2048]{2,1,0:T(8,128)(2,1)}, u32[]{:S(2)}) copy-start(bf16[2,256,2048]{2,1,0:T(8,128)(2,1)} %tok.1) | copy-start | bytes 6291460
  3.2 0.7 copy-start.2
  3.9 0.7 copy-start.3
  4.6 0.7 copy-start.4
